TPU v7x, 32 devices: a whole 2x2x4 slice. The times are simulated.
32 devices in a mesh: sp: 4 (over x, core), tp: 8 (over z, y).
Axes of the slice: x: 2, y: 2, z: 4, core: 2. Of those that a mesh axis runs over, the one named last changes fastest.
Arguments:
- latent: bfloat16 [512, 4096], P('sp', 'tp'), may hold values from -60 to 60
- context: bfloat16 [64, 4096], P('sp', 'tp'), may hold values from -6 to 6
- conditioning: bfloat16 [4096], P('sp'), may hold values from -6 to 6
- context_prompt_vector: bfloat16 [4096], P('sp'), may hold values from -6 to 6
- shift_matrix: bfloat16 [4096, 4096], P('tp', 'sp'), may hold values from -0.09375 to 0.09375
- scale_matrix: bfloat16 [4096, 4096], P('tp', 'sp'), may hold values from -0.09375 to 0.09375
- residual_gate_matrix: bfloat16 [4096, 4096], P('tp', 'sp'), may hold values from -0.09375 to 0.09375
- query_matrix: bfloat16 [2048, 4096], P('tp'), may hold values from -0.09375 to 0.09375
- key_matrix: bfloat16 [2048, 4096], P('tp'), may hold values from -0.09375 to 0.09375
- value_matrix: bfloat16 [4096, 4096], P('tp'), may hold values from -0.09375 to 0.09375
- gate_matrix: bfloat16 [4096, 4096], P('tp'), may hold values from -0.09375 to 0.09375
- decay_down_factor: bfloat16 [2, 4096, 16], replicated, may hold values from -0.09375 to 0.09375
- decay_up_factor: bfloat16 [2, 16, 2048], replicated, may hold values from -1.5 to 1.5
- decay_key_bias: float32 [2, 2048], replicated, may hold values from -0.5 to 7
- spike_log_decay: float32 [2, 512, 16], P(None, 'sp'), may hold values from -2.8 to 0
- output_gain: float32 [4096], P('tp'), may hold values from 0.1 to 1.9
- output_matrix: bfloat16 [4096, 4096], P('tp'), may hold values from -0.375 to 0.375
Outputs:
- mixed: bfloat16 [512, 4096], P('sp', 'tp')
All inputs are finite; a program needn't handle non-finite values.
Results may differ from a plain program's by a relative error of at most 0.013.
Values may be sent and summed in bfloat16 or wider, within the bound.
A program may use at most 64 MiB of HBM per device.

v0:
```python
import jax
import jax.numpy as jnp
from jax import lax
from jax.sharding import PartitionSpec as P

D = 4096
HEADS = 16
DK = 128
DECAY_RANK = 16
BLK = 64
VGROUP = 64
epsilon = 1e-05
gate_norm = 16.0
precise = lax.Precision.HIGHEST


def for_sending(value):

    def short(part):
        return part.astype(jnp.bfloat16) if part.dtype == jnp.float32 else part

    return jax.tree.map(short, value)


def from_partner(value, axis, distance):
    return lax.ppermute(value, axis, [(i, i ^ 1 << distance) for i in range(lax.axis_size(axis))])


def carried_in(value, axis, combine, identity, reverse):
    peers, index = (lax.axis_size(axis), lax.axis_index(axis))
    everything = jax.tree.map(
        lambda part, kind: lax.all_gather(part.astype(kind), axis),
        value,
        (jnp.bfloat16, jnp.bfloat16),
    )
    start = jax.tree.map(
        lambda part, zero: jnp.broadcast_to(jnp.asarray(zero, part.dtype), part.shape),
        value,
        identity,
    )

    def turn(k, before):
        at = peers - 1 - k if reverse else k
        reached = at > index if reverse else at < index
        new = combine(
            before, jax.tree.map(lambda part, own: part[at].astype(own.dtype), everything, value)
        )
        return jax.tree.map(lambda a, b: jnp.where(reached, a, b), new, before)

    return lax.fori_loop(0, peers, turn, start)


def linear(rows, weight):
    return lax.dot_general(
        rows, weight, (((1,), (1,)), ((), ())), preferred_element_type=jnp.float32
    )


def modulated(rows, row_sum, row_squares, shift_vec, scale_vec):
    rows_f = rows.astype(jnp.float32)
    mean_val = row_sum / D
    variance = row_squares / D - mean_val * mean_val
    return (
        (rows_f - mean_val) * lax.rsqrt(variance + epsilon) * (1.0 + scale_vec) + shift_vec
    ).astype(jnp.bfloat16)


def reverse_rows(array):
    return jnp.flip(array, axis=0)


def end_state(key_rows, value_rows, log_decay):
    cumulative = jnp.cumsum(log_decay, axis=0)
    totals = cumulative[-1]
    weighted = key_rows * jnp.exp(totals - cumulative)
    return (jnp.exp(totals), jnp.einsum("nhd,nhe->hde", weighted, value_rows, precision=precise))


def combine(earlier, later):
    return (earlier[0] * later[0], later[0][..., None] * earlier[1] + later[1])


def blockwise(queries, key_rows, value_rows, log_decay, carried, block_len):
    length, head_count, _ = queries.shape
    value_width = value_rows.shape[-1]
    blocks = length // block_len

    def shaped(array):
        return array.reshape(blocks, block_len, head_count, array.shape[-1])

    triangle = jnp.tril(jnp.ones((block_len, block_len), jnp.float32))

    def advance(state_now, inputs):
        block_q, block_k, block_v, block_a = inputs
        cumulative = jnp.cumsum(block_a, axis=0)
        block_end = cumulative[-1]
        query_dec = block_q * jnp.exp(cumulative)
        scores = (
            jnp.einsum("ihd,jhd->hij", query_dec, block_k * jnp.exp(-cumulative), precision=precise)
            * triangle
        )
        result = jnp.einsum("hij,jhe->ihe", scores, block_v, precision=precise)
        result = result + jnp.einsum("ihd,hde->ihe", query_dec, state_now, precision=precise)
        state_next = state_now * jnp.exp(block_end)[:, :, None] + jnp.einsum(
            "jhd,jhe->hde", block_k * jnp.exp(block_end - cumulative), block_v, precision=precise
        )
        return (state_next, result)

    _, outputs = lax.scan(
        advance, carried, (shaped(queries), shaped(key_rows), shaped(value_rows), shaped(log_decay))
    )
    return outputs.reshape(length, head_count, value_width)


def head_channels(pieces, per_head, tp_index):
    for bit_number in range(per_head.bit_length() - 1):
        partner = from_partner(
            (for_sending(pieces[0]), for_sending(pieces[1]), for_sending(pieces[2])),
            "tp",
            bit_number,
        )
        upper = tp_index // (1 << bit_number) % 2 == 1
        pieces = tuple(
            (
                jnp.where(
                    upper,
                    jnp.concatenate([theirs, mine], axis=1),
                    jnp.concatenate([mine, theirs], axis=1),
                )
                for mine, theirs in zip(pieces, partner)
            )
        )
    return pieces


def context_totals(fwd_growth, fwd_state, bwd_growth, bwd_state, identity):

    def absorb(carried, piece):
        return (combine(carried, piece), None)

    total_fwd, _ = lax.scan(absorb, identity, (fwd_growth, fwd_state))
    total_bwd, _ = lax.scan(absorb, identity, (bwd_growth, bwd_state), reverse=True)
    return (total_fwd, total_bwd)


def stored(array):
    return lax.optimization_barrier(array.astype(jnp.bfloat16))


def local(
    latent,
    context,
    conditioning,
    context_prompt_vector,
    shift_matrix,
    scale_matrix,
    residual_gate_matrix,
    query_matrix,
    key_matrix,
    value_matrix,
    gate_matrix,
    decay_down_factor,
    decay_up_factor,
    decay_key_bias,
    spike_log_decay,
    output_gain,
    output_matrix,
):
    tp_count = lax.axis_size("tp")
    tp_index = lax.axis_index("tp")
    per_head = max(tp_count // HEADS, 1)
    heads_per_shard = max(HEADS // tp_count, 1)
    leading_head = tp_index // per_head * heads_per_shard
    tok_rows = latent.shape[0]
    conds = jax.nn.silu(
        jnp.stack([conditioning, context_prompt_vector]).astype(jnp.float32)
    ).astype(jnp.bfloat16)
    shifts, scales, gates = lax.psum(
        (
            linear(conds, shift_matrix),
            linear(conds, scale_matrix),
            linear(conds, residual_gate_matrix),
        ),
        "sp",
    )
    down_both = jnp.concatenate([decay_down_factor[0].T, decay_down_factor[1].T], axis=0)
    lat_weights = (query_matrix, key_matrix, value_matrix, gate_matrix, down_both)
    ctx_weights = (key_matrix, value_matrix, down_both)
    lat_f = latent.astype(jnp.float32)
    ctx_f = context.astype(jnp.float32)
    lat_sum, lat_squares, ctx_sum, ctx_squares = lax.psum(
        (
            jnp.sum(lat_f, axis=1, keepdims=True),
            jnp.sum(lat_f * lat_f, axis=1, keepdims=True),
            jnp.sum(ctx_f, axis=1, keepdims=True),
            jnp.sum(ctx_f * ctx_f, axis=1, keepdims=True),
        ),
        "tp",
    )
    latent_normalized = modulated(latent, lat_sum, lat_squares, shifts[0], scales[0])
    normed_ctx = modulated(context, ctx_sum, ctx_squares, shifts[1], scales[1])
    lat_piece = lax.all_gather(latent_normalized, "tp", axis=1, tiled=True)
    ctx_piece = lax.all_gather(normed_ctx, "tp", axis=1, tiled=True)
    lat_new = tuple((linear(lat_piece, weight) for weight in lat_weights))
    ctx_new = tuple((linear(ctx_piece, weight) for weight in ctx_weights))
    query_part, key_part, value_part, gate_part, low_rank_part = lat_new
    ctx_key_part, ctx_value_part, ctx_low = ctx_new
    query_full, key_full, ctx_key_full = head_channels(
        (stored(query_part), stored(key_part), stored(ctx_key_part)), per_head, tp_index
    )

    def split_heads(rows, width):
        return rows.astype(jnp.float32).reshape(rows.shape[0], heads_per_shard, width)

    value_cols = value_part.shape[1] // heads_per_shard
    queries = split_heads(query_full, DK) * DK ** (-0.5)
    key_rows = split_heads(key_full, DK)
    ctx_keys = split_heads(ctx_key_full, DK)
    values_lat = split_heads(stored(value_part), value_cols)
    values_ctx = split_heads(stored(ctx_value_part), value_cols)
    gate_rows = stored(gate_part).astype(jnp.float32)

    def per_head_decay(low_rows, direction):
        up_part = lax.dynamic_slice_in_dim(
            decay_up_factor[direction], leading_head * DK, heads_per_shard * DK, 1
        ).astype(jnp.float32)
        bias_part = lax.dynamic_slice_in_dim(
            decay_key_bias[direction], leading_head * DK, heads_per_shard * DK, 0
        )
        pre_act = jnp.dot(low_rows, up_part, precision=precise) + bias_part
        return (jax.nn.log_sigmoid(pre_act) / gate_norm).reshape(
            low_rows.shape[0], heads_per_shard, DK
        )

    decay_spikes = lax.dynamic_slice_in_dim(spike_log_decay, leading_head, heads_per_shard, 2)
    latent_forward = per_head_decay(low_rank_part[:, :DECAY_RANK], 0) + decay_spikes[0][:, :, None]
    latent_backward = per_head_decay(low_rank_part[:, DECAY_RANK:], 1) + decay_spikes[1][:, :, None]
    ctx_fwd = per_head_decay(ctx_low[:, :DECAY_RANK], 0)
    ctx_bwd = per_head_decay(ctx_low[:, DECAY_RANK:], 1)
    cf_growth, cf_state = end_state(ctx_keys, values_ctx, ctx_fwd)
    cb_growth, cb_state = end_state(
        reverse_rows(ctx_keys), reverse_rows(values_ctx), reverse_rows(ctx_bwd)
    )
    lf_growth, lf_state = end_state(key_rows, values_lat, latent_forward)
    lb_growth, lb_state = end_state(
        reverse_rows(key_rows), reverse_rows(values_lat), reverse_rows(latent_backward)
    )
    identity = (
        jnp.ones((heads_per_shard, DK), jnp.float32),
        jnp.zeros((heads_per_shard, DK, value_cols), jnp.float32),
    )
    ctx_gathered = (
        lax.all_gather(cf_growth[None].astype(jnp.bfloat16), "sp", axis=0, tiled=True).astype(
            jnp.float32
        ),
        lax.all_gather(cf_state[None].astype(jnp.bfloat16), "sp", axis=0, tiled=True).astype(
            jnp.float32
        ),
        lax.all_gather(cb_growth[None].astype(jnp.bfloat16), "sp", axis=0, tiled=True).astype(
            jnp.float32
        ),
        lax.all_gather(cb_state[None].astype(jnp.bfloat16), "sp", axis=0, tiled=True).astype(
            jnp.float32
        ),
    )
    total_fwd, total_bwd = context_totals(
        ctx_gathered[0], ctx_gathered[1], ctx_gathered[2], ctx_gathered[3], identity
    )
    prefix = carried_in((lf_growth, lf_state), "sp", combine, identity, False)
    suffix = carried_in((lb_growth, lb_state), "sp", combine, identity, True)
    start_fwd = combine(total_fwd, prefix)[1]
    start_bwd = combine(total_bwd, suffix)[1]
    zero_state = jnp.zeros((heads_per_shard, DK, value_cols), jnp.float32)

    def direction_out(query_rows, key_list, value_list, log_decay, start_state):
        local_part = blockwise(query_rows, key_list, value_list, log_decay, zero_state, BLK)
        reach = query_rows * jnp.exp(jnp.cumsum(log_decay, axis=0))
        return local_part + jnp.einsum("nhd,hde->nhe", reach, start_state, precision=precise)

    out_fwd = direction_out(queries, key_rows, values_lat, latent_forward, start_fwd)
    out_bwd = reverse_rows(
        direction_out(
            reverse_rows(queries),
            reverse_rows(key_rows),
            reverse_rows(values_lat),
            reverse_rows(latent_backward),
            start_bwd,
        )
    )
    grouped = (out_fwd + out_bwd).reshape(tok_rows, -1, VGROUP)
    grouped = grouped * lax.rsqrt(jnp.mean(grouped * grouped, axis=-1, keepdims=True) + epsilon)
    heads_out = (grouped.reshape(tok_rows, -1) * output_gain * jax.nn.silu(gate_rows)).astype(
        jnp.bfloat16
    )
    branch = linear(lax.all_gather(heads_out, "tp", axis=1, tiled=True), output_matrix)
    return (latent.astype(jnp.float32) + gates[0] * branch).astype(jnp.bfloat16)


def solution(mesh):
    placed = (
        P("sp", "tp"),
        P("sp", "tp"),
        P("sp"),
        P("sp"),
        P("tp", "sp"),
        P("tp", "sp"),
        P("tp", "sp"),
        P("tp", None),
        P("tp", None),
        P("tp", None),
        P("tp", None),
        P(),
        P(),
        P(),
        P(None, "sp", None),
        P("tp"),
        P("tp", None),
    )
    return jax.shard_map(
        local, mesh=mesh, in_specs=placed, out_specs=P("sp", "tp"), check_vma=False
    )
```

profile of v0, /device:TPU:0, one launch (start us, length us, event | category | flops | bytes accessed | tf_op | source)
XLA Modules:
  0.0 266.8 jit_solution(12194387579442730119)
XLA Ops:
  14.8 13.2 %all-reduce.1 = (f32[2,512]{1,0:T(2,128)S(1)}, f32[2,512]{1,0:T(2,128)S(1)}, f32[2,512]{1,0:T(2,128)}) all-reduce(f32[2,512]{1,0:T(2,128)S(1)} %fusion.121, f32[2,512]{1,0:T(2,128)S(1)} %fusion.123, f32[2,512]{1,0:T(2,128)S(1)} %fusion.125), channel_id=1, replica_groups=mesh['sp'=4,'tp'=8] {'sp'}, use_global_device_ids=true, to_apply=%region_6.7 | all-reduce | flops 3072 | bytes 24576 | tf_op jit(solution)/shard_map/psum | solution.py:178
  28.0 21.7 %all-reduce = (f32[128,1]{0,1:T(1,128)S(1)}, f32[128,1]{0,1:T(1,128)S(1)}, f32[16,1]{0,1:T(1,128)S(1)}, f32[16,1]{0,1:T(1,128)S(1)}) all-reduce(f32[128,1]{0,1:T(1,128)S(1)} %bitcast.291, f32[128,1]{0,1:T(1,128)S(1)} %bitcast.290, f32[16,1]{0,1:T(1,128)S(1)} %bitcast.293, f32[16,1]{0,1:T(1,128)S(1)} %bitcast.292), channel_id=1, replica_groups=mesh['sp'=4,'tp'=8] {'tp'}, use_global_device_ids=true, to_apply=%region_4.5 | all-reduce | flops 288 | bytes 2304 | tf_op jit(solution)/shard_map/psum | solution.py:191
  49.7 1.7 fusion.62
  53.5 31.0 %all_gather.45 = bf16[16,4096]{1,0:T(8,128)(2,1)S(1)} all-gather(bf16[16,512]{1,0:T(8,128)(2,1)S(1)} %fusion.89), channel_id=1, replica_groups=mesh['sp'=4,'tp'=8] {'tp'}, dimensions={1}, use_global_device_ids=true | all-gather | bytes 147456 | tf_op jit(solution)/shard_map/all_gather | solution.py:203
  84.9 3.4 %convolution_convert_fusion.8 = bf16[16,512]{1,0:T(8,128)(2,1)S(1)} fusion(bf16[16,4096]{1,0:T(8,128)(2,1)S(1)} %all_gather.45, bf16[512,4096]{1,0:T(8,128)(2,1)} %param.38), kind=kOutput, calls=%fused_computation.96 | convolution fusion | flops 67117056 | bytes 4341760 | tf_op jit(solution)/shard_map/dot_general | solution.py:54
  89.8 5.1 %all_gather.46 = bf16[4,2,128]{2,1,0:T(2,128)(2,1)S(1)} all-gather(bf16[1,2,128]{2,1,0:T(2,128)(2,1)S(1)} %get-tuple-element.728), channel_id=1, replica_groups=mesh['sp'=4,'tp'=8] {'sp'}, dimensions={0}, use_global_device_ids=true | all-gather | bytes 2560 | tf_op jit(solution)/shard_map/all_gather | solution.py:253
  95.8 7.3 %all-gather.1 = bf16[8,128,256]{2,1,0:T(8,128)(2,1)S(1)} all-gather(bf16[2,128,256]{2,1,0:T(8,128)(2,1)S(1)} %convolution_convert_fusion.5), channel_id=3, replica_groups=mesh['sp'=4,'tp'=8] {'sp'}, dimensions={0}, use_global_device_ids=true | all-gather | bytes 655360 | tf_op jit(solution)/shard_map/all_gather | solution.py:256
  106.9 5.0 %all_gather.51 = bf16[4,2,128]{2,1,0:T(2,128)(2,1)S(1)} all-gather(bf16[1,2,128]{2,1,0:T(2,128)(2,1)S(1)} %get-tuple-element.734), channel_id=1, replica_groups=mesh['sp'=4,'tp'=8] {'sp'}, dimensions={0}, use_global_device_ids=true | all-gather | bytes 2560 | tf_op jit(solution)/shard_map/all_gather | solution.py:259
  113.8 7.5 %all-gather.3 = bf16[8,128,256]{2,1,0:T(8,128)(2,1)S(1)} all-gather(bf16[2,128,256]{2,1,0:T(8,128)(2,1)S(1)} %convolution_convert_fusion.4), channel_id=5, replica_groups=mesh['sp'=4,'tp'=8] {'sp'}, dimensions={0}, use_global_device_ids=true | all-gather | bytes 655360 | tf_op jit(solution)/shard_map/all_gather | solution.py:262
  122.4 4.4 %while.91 = (s32[]{:T(128)}, f32[2,128,256]{2,1,0:T(8,128)S(1)}, f32[4,2,128]{2,1,0:T(2,128)S(1)}, f32[4,2,128,256]{3,2,1,0:T(8,128)}, s32[]{:T(128)}, /*index=5*/s32[]{:T(128)}, s32[]{:T(128)}) while((s32[]{:T(128)}, f32[2,128,256]{2,1,0:T(8,128)S(1)}, f32[4,2,128]{2,1,0:T(2,128)S(1)}, f32[4,2,128,256]{3,2,1,0:T(8,128)}, ...), condition=%wide.region_28.29_spmd.clone, body=%wide.region_27.28_spmd.clone.sunk | while | flops 196612 | bytes 789619 | solution.py:142
  127.5 1.8 fusion.70
  129.3 1.7 fusion.74
  133.5 2.1 convolution_convert_fusion.7
  137.0 3.7 %convolution_convert_fusion.2 = bf16[128,512]{1,0:T(8,128)(2,1)S(1)} fusion(bf16[128,4096]{1,0:T(8,128)(2,1)S(1)} %copy-done.1, bf16[512,4096]{1,0:T(8,128)(2,1)} %param.38), kind=kOutput, calls=%fused_computation.85 | convolution fusion | flops 536936448 | bytes 5373952 | tf_op jit(solution)/shard_map/dot_general | solution.py:54
  142.3 3.1 %convolution_convert_fusion.6 = bf16[128,256]{1,0:T(8,128)(2,1)} fusion(bf16[128,4096]{1,0:T(8,128)(2,1)S(1)} %copy-done.1, bf16[256,4096]{1,0:T(8,128)(2,1)} %param.36), kind=kOutput, calls=%fused_computation.94 | convolution fusion | flops 268468224 | bytes 3211264 | tf_op jit(solution)/shard_map/dot_general | solution.py:54
  148.4 4.4 %convolution_convert_fusion = bf16[128,512]{1,0:T(8,128)(2,1)} fusion(bf16[128,4096]{1,0:T(8,128)(2,1)S(1)} %copy-done.1, bf16[512,4096]{1,0:T(8,128)(2,1)} %param.39), kind=kOutput, calls=%fused_computation.83 | convolution fusion | flops 536936448 | bytes 5373952 | tf_op jit(solution)/shard_map/dot_general | solution.py:54
  158.9 2.3 exponential_multiply_fusion.2
  161.9 5.9 %while.89 = (s32[]{:T(128)}, f32[2,128,256]{2,1,0:T(8,128)S(1)}, f32[2,64,2,256]{3,1,0,2:T(8,128)}, f32[2,64,2,128]{3,2,1,0:T(2,128)S(1)}, f32[2,64,2,128]{3,2,1...) while((s32[]{:T(128)}, f32[2,128,256]{2,1,0:T(8,128)S(1)}, ...), condition=%wide.region_22.23_spmd.clone, body=%wide.region_20.22_spmd.clone.sunk | while | flops 139837440 | bytes 2366588 | solution.py:109
  167.8 1.9 copy.96
  169.7 5.1 %all_gather.48 = bf16[4,2,128]{2,1,0:T(2,128)(2,1)S(1)} all-gather(bf16[1,2,128]{2,1,0:T(2,128)(2,1)} %get-tuple-element.724), channel_id=1, replica_groups=mesh['sp'=4,'tp'=8] {'sp'}, dimensions={0}, use_global_device_ids=true | all-gather | bytes 2560 | tf_op jit(solution)/shard_map/all_gather | solution.py:32
  176.1 7.9 %all-gather.2 = bf16[8,128,256]{2,1,0:T(8,128)(2,1)} all-gather(bf16[2,128,256]{2,1,0:T(8,128)(2,1)S(1)} %convolution_convert_fusion.1), channel_id=4, replica_groups=mesh['sp'=4,'tp'=8] {'sp'}, dimensions={0}, use_global_device_ids=true | all-gather | bytes 655360 | tf_op jit(solution)/shard_map/all_gather | solution.py:32
  184.0 4.4 %while.90 = (s32[]{:T(128)}, f32[2,128]{1,0:T(2,128)S(1)}, f32[2,128,256]{2,1,0:T(8,128)S(1)}, s32[]{:T(128)}, bf16[4,2,128]{2,1,0:T(2,128)(2,1)S(1)}, /*index=5...) while((s32[]{:T(128)}, f32[2,128]{1,0:T(2,128)S(1)}, ...), condition=%wide.region_25.26_spmd.clone, body=%wide.region_24.25_spmd.clone.sunk | while | flops 328968 | bytes 660669 | solution.py:50
  188.4 2.4 fusion.46
  190.8 3.1 %rev.38 = f32[128,2,256]{0,2,1:T(8,128)} reverse(f32[128,2,256]{0,2,1:T(8,128)} %fusion.46), dimensions={0} | reverse | bytes 524288 | tf_op jit(solution)/shard_map/jit(_flip)/rev | solution.py:69
  195.8 4.3 %while.86 = (s32[]{:T(128)}, f32[2,128,256]{2,1,0:T(8,128)S(1)}, f32[2,64,2,256]{3,1,0,2:T(8,128)}, f32[2,64,2,128]{3,2,1,0:T(2,128)S(1)}, f32[2,64,2,128]{3,2,1...) while((s32[]{:T(128)}, f32[2,128,256]{2,1,0:T(8,128)S(1)}, ...), condition=%wide.region_9.10_spmd.clone, body=%wide.region_7.9_spmd.clone.sunk | while | flops 139837440 | bytes 2594944 | solution.py:109
  200.1 1.8 copy.86
  201.9 5.0 %all_gather.42 = bf16[4,2,128]{2,1,0:T(2,128)(2,1)S(1)} all-gather(bf16[1,2,128]{2,1,0:T(2,128)(2,1)S(1)} %get-tuple-element.720), channel_id=1, replica_groups=mesh['sp'=4,'tp'=8] {'sp'}, dimensions={0}, use_global_device_ids=true | all-gather | bytes 2560 | tf_op jit(solution)/shard_map/all_gather | solution.py:32
  207.3 7.6 %all-gather = bf16[8,128,256]{2,1,0:T(8,128)(2,1)S(1)} all-gather(bf16[2,128,256]{2,1,0:T(8,128)(2,1)S(1)} %convolution_convert_fusion.3), channel_id=2, replica_groups=mesh['sp'=4,'tp'=8] {'sp'}, dimensions={0}, use_global_device_ids=true | all-gather | bytes 655360 | tf_op jit(solution)/shard_map/all_gather | solution.py:32
  215.7 1.7 fusion.130
  217.8 1.7 fusion.68
  219.5 35.8 %all-gather.9.cloned.1.call-done = bf16[128,4096]{1,0:T(8,128)(2,1)} async-done(((bf16[128,512]{1,0:T(8,128)(2,1)}), bf16[128,4096]{1,0:T(8,128)(2,1)}) %all-gather.9.cloned.1.call-update) | async-done | bytes 1048592 | tf_op jit(solution)/shard_map/all_gather | solution.py:295
  255.3 4.7 %fusion.50 = bf16[128,512]{1,0:T(8,128)(2,1)} fusion(bf16[128,4096]{1,0:T(8,128)(2,1)} %all-gather.9.cloned.1.call-done, bf16[512,4096]{1,0:T(8,128)(2,1)} %param.45, bf16[128,512]{1,0:T(8,128)(2,1)S(1)} %copy-done.11, f32[512]{0:T(512)S(1)} %bitcast.285), kind=kOutput, calls=%fused_computation.87 | convolution fusion | flops 537133056 | bytes 5507072 | tf_op jit(solution)/shard_map/dot_general | solution.py:54
  (210 shorter events, 60.2 us)
Async XLA Ops:
  6.5 82.4 %copy-start = (bf16[256,4096]{1,0:T(8,128)(2,1)S(1)}, bf16[256,4096]{1,0:T(8,128)(2,1)}, u32[]{:S(2)}) copy-start(bf16[256,4096]{1,0:T(8,128)(2,1)} %param.37) | copy-start | bytes 6291460
  6.5 46.8 %copy-start.17 = (bf16[16,512]{1,0:T(8,128)(2,1)S(1)}, bf16[16,512]{1,0:T(8,128)(2,1)}, u32[]{:S(2)}) copy-start(bf16[16,512]{1,0:T(8,128)(2,1)} %param.30) | copy-start | bytes 49156
  6.5 46.7 %copy-start.16 = (bf16[2,16,2048]{2,1,0:T(8,128)(2,1)S(1)}, bf16[2,16,2048]{2,1,0:T(8,128)(2,1)}, u32[]{:S(2)}) copy-start(bf16[2,16,2048]{2,1,0:T(8,128)(2,1)} %param.41) | copy-start | bytes 393220
  6.5 121.0 %all-gather.7.cloned.1.call-start = ((), (), s32[]{:S(2)}) async-start(), calls=%async_computation | async-start | bytes 1179648 | tf_op jit(solution)/shard_map/all_gather | solution.py:202
  51.4 203.9 %all-gather.9.cloned.1.call-start = ((), (), s32[]{:S(2)}) async-start(), calls=%async_computation.1 | async-start | bytes 1179648 | tf_op jit(solution)/shard_map/all_gather | solution.py:295
  53.3 49.8 %copy-start.15 = (bf16[16,4096]{1,0:T(8,128)(2,1)}, bf16[16,4096]{1,0:T(8,128)(2,1)S(1)}, u32[]{:S(2)}) copy-start(bf16[16,4096]{1,0:T(8,128)(2,1)S(1)} %get-tuple-element.713) | copy-start | bytes 393220
  53.3 49.8 %copy-start.18 = (bf16[1,16,2048]{2,1,0:T(8,128)(2,1)}, bf16[1,16,2048]{2,1,0:T(8,128)(2,1)S(1)}, u32[]{:S(2)}) copy-start(bf16[1,16,2048]{2,1,0:T(8,128)(2,1)S(1)} %get-tuple-element.721) | copy-start | bytes 196612
  53.3 49.8 %copy-start.19 = (bf16[1,16,2048]{2,1,0:T(8,128)(2,1)}, bf16[1,16,2048]{2,1,0:T(8,128)(2,1)S(1)}, u32[]{:S(2)}) copy-start(bf16[1,16,2048]{2,1,0:T(8,128)(2,1)S(1)} %get-tuple-element.722) | copy-start | bytes 196612
  84.4 5.4 %copy-start.22 = (f32[1,256]{1,0:T(1,128)}, f32[1,256]{1,0:T(1,128)S(1)}, u32[]{:S(2)}) copy-start(f32[1,256]{1,0:T(1,128)S(1)} %get-tuple-element.747) | copy-start | bytes 3076
  103.9 0.8 copy-start.3
  126.8 0.7 copy-start.5
  127.5 9.4 %copy-start.1 = (bf16[128,4096]{1,0:T(8,128)(2,1)S(1)}, bf16[128,4096]{1,0:T(8,128)(2,1)}, u32[]{:S(2)}) copy-start(bf16[128,4096]{1,0:T(8,128)(2,1)} %all-gather.7.cloned.1.call-done) | copy-start | bytes 3145732
  152.8 9.1 %copy-start.2 = (f32[2,128,256]{2,1,0:T(8,128)S(1)}, f32[2,128,256]{2,1,0:T(8,128)}, u32[]{:S(2)}) copy-start(f32[2,128,256]{2,1,0:T(8,128)} %custom-call.4) | copy-start | bytes 786436
  161.9 22.1 %copy-start.8 = (f32[2,128,256]{2,1,0:T(8,128)S(1)}, f32[2,128,256]{2,1,0:T(8,128)}, u32[]{:S(2)}) copy-start(f32[2,128,256]{2,1,0:T(8,128)} %custom-call.6) | copy-start | bytes 786436
  167.8 20.6 %copy-start.6 = (f32[2,128,256]{2,1,0:T(8,128)S(1)}, f32[2,128,256]{2,1,0:T(8,128)}, u32[]{:S(2)}) copy-start(f32[2,128,256]{2,1,0:T(8,128)} %copy-done.5) | copy-start | bytes 786436
  167.8 28.0 %copy-start.9 = (f32[2,64,2,256]{3,2,1,0:T(2,128)S(1)}, f32[2,64,2,256]{3,2,1,0:T(2,128)}, u32[]{:S(2)}) copy-start(f32[2,64,2,256]{3,2,1,0:T(2,128)} %reshape_reshape.7) | copy-start | bytes 786436
  176.1 17.8 %copy-start.14 = (f32[128,256]{1,0:T(8,128)S(1)}, f32[128,256]{1,0:T(8,128)}, u32[]{:S(2)}) copy-start(f32[128,256]{1,0:T(8,128)} %broadcast_multiply_fusion) | copy-start | bytes 393220
  176.1 19.7 %copy-start.10 = (f32[2,64,2,128]{3,2,1,0:T(2,128)S(1)}, f32[2,64,2,128]{3,2,1,0:T(2,128)}, u32[]{:S(2)}) copy-start(f32[2,64,2,128]{3,2,1,0:T(2,128)} %reshape_reshape.6) | copy-start | bytes 393220
  195.8 11.2 %copy-start.13 = (f32[128,2,128]{2,1,0:T(2,128)S(1)}, f32[128,2,128]{2,1,0:T(2,128)}, u32[]{:S(2)}) copy-start(f32[128,2,128]{2,1,0:T(2,128)} %get-tuple-element.717) | copy-start | bytes 393220
  195.8 19.2 %copy-start.7 = (f32[2,128,256]{2,1,0:T(8,128)S(1)}, f32[2,128,256]{2,1,0:T(8,128)}, u32[]{:S(2)}) copy-start(f32[2,128,256]{2,1,0:T(8,128)} %custom-call.2) | copy-start | bytes 786436
  200.1 15.6 %copy-start.4 = (f32[2,128,256]{2,1,0:T(8,128)S(1)}, f32[2,128,256]{2,1,0:T(8,128)}, u32[]{:S(2)}) copy-start(f32[2,128,256]{2,1,0:T(8,128)} %copy-done.3) | copy-start | bytes 786436
  200.1 17.7 %copy-start.20 = (f32[512]{0:T(512)S(1)}, f32[512]{0:T(512)}, u32[]{:S(2)}) copy-start(f32[512]{0:T(512)} %param.44) | copy-start | bytes 6148
  207.3 8.4 %copy-start.12 = (f32[128,2,256]{0,2,1:T(8,128)S(1)}, f32[128,2,256]{0,2,1:T(8,128)}, u32[]{:S(2)}) copy-start(f32[128,2,256]{0,2,1:T(8,128)} %rev.38) | copy-start | bytes 786436
  207.3 12.2 %copy-start.21 = (f32[2,512]{1,0:T(2,128)S(1)}, f32[2,512]{1,0:T(2,128)}, u32[]{:S(2)}) copy-start(f32[2,512]{1,0:T(2,128)} %get-tuple-element.705) | copy-start | bytes 12292
  207.3 47.9 %copy-start.11 = (bf16[128,512]{1,0:T(8,128)(2,1)S(1)}, bf16[128,512]{1,0:T(8,128)(2,1)}, u32[]{:S(2)}) copy-start(bf16[128,512]{1,0:T(8,128)(2,1)} %param.29) | copy-start | bytes 393220
Sparse Core Ops, SparseCore 0:
  51.5 35.1 all-gather.6
  219.6 35.6 all-gather.8
where the time goes:
time: 269 us; the launch traced here: 267 us
  blocking collectives  116 us (43%)
  matrix products  46.5 us (17%)
  waiting for transfers between devices  35.8 us (13%)
  other arithmetic  28.5 us (11%)
  local copies, waits for them, and re-layouts  25 us (9%)
  between operations  13.9 us (5%)
    all_gather x1, waiting for transfers between devices, local(): lax.all_gather(heads_out, 'tp', axis=1, tiled=True)  35.8 us
    all_gather x1, blocking collectives, local(): ctx_piece = lax.all_gather(normed_ctx, 'tp', axis=1, tiled=True)  31 us
    dot_general x12, matrix products, linear(): lax.dot_general(rows, weight, (((1,), (1,)), ((), ())), preferred_element...  28.7 us
    all_gather x4, blocking collectives, carried_in(): lax.all_gather(part.astype(kind), axis)  25.6 us
    psum x1, blocking collectives, local(): lax.psum((jnp.sum(lat_f, axis=1, keepdims=True), jnp.sum(lat_f * lat_f, a...  21.7 us
    psum x1, blocking collectives, local(): lax.psum((linear(conds, shift_matrix), linear(conds, scale_matrix), linea...  13.2 us
    all_gather x1, blocking collectives, local(): lax.all_gather(cb_state[None].astype(jnp.bfloat16), 'sp', axis=0, tiled=T...  7.46 us
    all_gather x1, blocking collectives, local(): lax.all_gather(cf_state[None].astype(jnp.bfloat16), 'sp', axis=0, tiled=T...  7.28 us
  transfers between devices with their start and end apart: 2, of which 1 were waited for; matrix products, arithmetic and copies ran while one was open for 7% of the time, Pallas kernels for 0%

commit v1 on v0

--- a/solution.py
+++ b/solution.py
@@ -12,6 +12,12 @@
 epsilon = 1e-05
 gate_norm = 16.0
 precise = lax.Precision.HIGHEST
+
+
+def _play_lots_all(work_x):
+    side_arr = jnp.stack([work_x] * lax.axis_size("tp"))
+    after = lax.all_to_all(side_arr, axis_name="tp", split_axis=0, concat_axis=0)
+    return jnp.concatenate(after, axis=1)
 
 
 def for_sending(value):
@@ -200,7 +206,7 @@
     latent_normalized = modulated(latent, lat_sum, lat_squares, shifts[0], scales[0])
     normed_ctx = modulated(context, ctx_sum, ctx_squares, shifts[1], scales[1])
     lat_piece = lax.all_gather(latent_normalized, "tp", axis=1, tiled=True)
-    ctx_piece = lax.all_gather(normed_ctx, "tp", axis=1, tiled=True)
+    ctx_piece = _play_lots_all(normed_ctx)
     lat_new = tuple((linear(lat_piece, weight) for weight in lat_weights))
     ctx_new = tuple((linear(ctx_piece, weight) for weight in ctx_weights))
     query_part, key_part, value_part, gate_part, low_rank_part = lat_new

time: 269 us -> 249 us (0.926)
  blocking collectives: 116 us -> 85.4 us
  waiting for transfers between devices: 35.8 us -> 40.3 us
  other arithmetic: 28.5 us -> 32.8 us
  starting transfers between devices: 0.04 us -> 3.44 us
    all_gather x1 -> x0, blocking collectives: 31 us -> none  [local(): ctx_piece = lax.all_gather(normed_ctx, 'tp', axis=1, tiled=True)]
    add x8, other arithmetic: 4.77 us -> 8.56 us  [combine(): return (earlier[0] * later[0], later[0][..., None] * earlier[1] + later[1])]
    all_to_all x0 -> x1, waiting for transfers between devices: none -> 3.45 us  [_play_lots_all(): lax.all_to_all(side_arr, axis_name='tp', split_axis=0, concat_axis=0)]
    all_to_all x0 -> x1, starting transfers between devices: none -> 3.37 us  [_play_lots_all(): lax.all_to_all(side_arr, axis_name='tp', split_axis=0, concat_axis=0)]
  transfers between devices with their start and end apart: 2 -> 3, of which waited for: 1 -> 2; matrix products, arithmetic and copies ran while one was open for 7% -> 9% of each run, Pallas kernels for 0% -> 0%
where the time goes in v1:
time: 249 us; the launch traced here: 248 us
  blocking collectives  85.4 us (34%)
  matrix products  47.2 us (19%)
  waiting for transfers between devices  40.3 us (16%)
  other arithmetic  32.8 us (13%)
  local copies, waits for them, and re-layouts  23.8 us (10%)
  between operations  13.9 us (6%)
  starting transfers between devices  3.44 us (1%)
    all_gather x1, waiting for transfers between devices, local(): lax.all_gather(heads_out, 'tp', axis=1, tiled=True)  36.8 us
    dot_general x12, matrix products, linear(): lax.dot_general(rows, weight, (((1,), (1,)), ((), ())), preferred_element...  28.7 us
    all_gather x4, blocking collectives, carried_in(): lax.all_gather(part.astype(kind), axis)  25.6 us
    psum x1, blocking collectives, local(): lax.psum((jnp.sum(lat_f, axis=1, keepdims=True), jnp.sum(lat_f * lat_f, a...  21.7 us
    psum x1, blocking collectives, local(): lax.psum((linear(conds, shift_matrix), linear(conds, scale_matrix), linea...  13.2 us
    add x8, other arithmetic, combine(): return (earlier[0] * later[0], later[0][..., None] * earlier[1] + later[1])  8.56 us
    all_gather x1, blocking collectives, local(): lax.all_gather(cb_state[None].astype(jnp.bfloat16), 'sp', axis=0, tiled=T...  7.45 us
    all_gather x1, blocking collectives, local(): lax.all_gather(cf_state[None].astype(jnp.bfloat16), 'sp', axis=0, tiled=T...  7.27 us
  transfers between devices with their start and end apart: 3, of which 2 were waited for; matrix products, arithmetic and copies ran while one was open for 9% of the time, Pallas kernels for 0%

profile of v1, /device:TPU:0, one launch (start us, length us, event | category | flops | bytes accessed | tf_op | source)
XLA Modules:
  0.0 247.5 jit_solution(16109635681564169563)
XLA Ops:
  14.8 13.2 %all-reduce.1 = (f32[2,512]{1,0:T(2,128)S(1)}, f32[2,512]{1,0:T(2,128)S(1)}, f32[2,512]{1,0:T(2,128)}) all-reduce(f32[2,512]{1,0:T(2,128)S(1)} %fusion.121, f32[2,512]{1,0:T(2,128)S(1)} %fusion.123, f32[2,512]{1,0:T(2,128)S(1)} %fusion.125), channel_id=1, replica_groups=mesh['sp'=4,'tp'=8] {'sp'}, use_global_device_ids=true, to_apply=%region_6.7 | all-reduce | flops 3072 | bytes 24576 | tf_op jit(solution)/shard_map/psum | solution.py:184
  28.0 21.7 %all-reduce = (f32[128,1]{0,1:T(1,128)S(1)}, f32[128,1]{0,1:T(1,128)S(1)}, f32[16,1]{0,1:T(1,128)S(1)}, f32[16,1]{0,1:T(1,128)S(1)}) all-reduce(f32[128,1]{0,1:T(1,128)S(1)} %bitcast.298, f32[128,1]{0,1:T(1,128)S(1)} %bitcast.297, f32[16,1]{0,1:T(1,128)S(1)} %bitcast.300, f32[16,1]{0,1:T(1,128)S(1)} %bitcast.299), channel_id=1, replica_groups=mesh['sp'=4,'tp'=8] {'tp'}, use_global_device_ids=true, to_apply=%region_4.5 | all-reduce | flops 288 | bytes 2304 | tf_op jit(solution)/shard_map/psum | solution.py:197
  49.7 1.7 fusion.62
  52.9 3.4 %all-to-all-start = ((bf16[8,16,512]{2,1,0:T(8,128)(2,1)}), bf16[8,16,512]{2,1,0:T(8,128)(2,1)S(1)}, u32[]{:S(2)}, u32[]{:S(2)}) async-start(bf16[8,16,512]{2,1,0:T(8,128)(2,1)} %stack.11), calls=%async_computation | async-start | bytes 262144 | tf_op jit(solution)/shard_map/all_to_all | solution.py:19
  60.1 3.5 %all-to-all-done = bf16[8,16,512]{2,1,0:T(8,128)(2,1)S(1)} async-done(((bf16[8,16,512]{2,1,0:T(8,128)(2,1)}), bf16[8,16,512]{2,1,0:T(8,128)(2,1)S(1)}, u32[]{:S(2)}, u32[]{:S(2)}) %all-to-all-start) | async-done | bytes 131104 | tf_op jit(solution)/shard_map/all_to_all | solution.py:19
  64.7 3.4 %convolution_convert_fusion.8 = bf16[16,512]{1,0:T(8,128)(2,1)S(1)} fusion(bf16[16,4096]{1,0:T(8,128)(2,1)S(1)} %bitcast.278, bf16[512,4096]{1,0:T(8,128)(2,1)} %param.38), kind=kOutput, calls=%fused_computation.96 | convolution fusion | flops 67117056 | bytes 4341760 | tf_op jit(solution)/shard_map/dot_general | solution.py:60
  69.7 5.1 %all_gather.42 = bf16[4,2,128]{2,1,0:T(2,128)(2,1)S(1)} all-gather(bf16[1,2,128]{2,1,0:T(2,128)(2,1)S(1)} %get-tuple-element.728), channel_id=1, replica_groups=mesh['sp'=4,'tp'=8] {'sp'}, dimensions={0}, use_global_device_ids=true | all-gather | bytes 2560 | tf_op jit(solution)/shard_map/all_gather | solution.py:259
  75.2 7.3 %all-gather.1 = bf16[8,128,256]{2,1,0:T(8,128)(2,1)S(1)} all-gather(bf16[2,128,256]{2,1,0:T(8,128)(2,1)S(1)} %convolution_convert_fusion.5), channel_id=3, replica_groups=mesh['sp'=4,'tp'=8] {'sp'}, dimensions={0}, use_global_device_ids=true | all-gather | bytes 655360 | tf_op jit(solution)/shard_map/all_gather | solution.py:262
  83.5 4.4 %while.88 = (s32[]{:T(128)}, f32[2,128,256]{2,1,0:T(8,128)S(1)}, f32[4,2,128]{2,1,0:T(2,128)S(1)}, f32[4,2,128,256]{3,2,1,0:T(8,128)}, s32[]{:T(128)}, /*index=5*/s32[]{:T(128)}) while((s32[]{:T(128)}, f32[2,128,256]{2,1,0:T(8,128)S(1)}, f32[4,2,128]{2,1,0:T(2,128)S(1)}, f32[4,2,128,256]{3,2,1,0:T(8,128)}, s32[]{:T(128)}, ...), condition=%wide.region_19.20_spmd.clone, body=%wide.region_18.19_spmd.clone.sunk | while | flops 196611 | bytes 789599 | solution.py:147
  88.0 5.1 %all_gather.47 = bf16[4,2,128]{2,1,0:T(2,128)(2,1)S(1)} all-gather(bf16[1,2,128]{2,1,0:T(2,128)(2,1)S(1)} %get-tuple-element.734), channel_id=1, replica_groups=mesh['sp'=4,'tp'=8] {'sp'}, dimensions={0}, use_global_device_ids=true | all-gather | bytes 2560 | tf_op jit(solution)/shard_map/all_gather | solution.py:265
  93.5 7.5 %all-gather.3 = bf16[8,128,256]{2,1,0:T(8,128)(2,1)S(1)} all-gather(bf16[2,128,256]{2,1,0:T(8,128)(2,1)S(1)} %convolution_convert_fusion.4), channel_id=5, replica_groups=mesh['sp'=4,'tp'=8] {'sp'}, dimensions={0}, use_global_device_ids=true | all-gather | bytes 655360 | tf_op jit(solution)/shard_map/all_gather | solution.py:268
  102.1 4.4 %while.91 = (s32[]{:T(128)}, f32[2,128,256]{2,1,0:T(8,128)S(1)}, f32[4,2,128]{2,1,0:T(2,128)S(1)}, f32[4,2,128,256]{3,2,1,0:T(8,128)}, s32[]{:T(128)}, /*index=5*/s32[]{:T(128)}, s32[]{:T(128)}) while((s32[]{:T(128)}, f32[2,128,256]{2,1,0:T(8,128)S(1)}, f32[4,2,128]{2,1,0:T(2,128)S(1)}, f32[4,2,128,256]{3,2,1,0:T(8,128)}, ...), condition=%wide.region_28.29_spmd.clone, body=%wide.region_27.28_spmd.clone.sunk | while | flops 196612 | bytes 789619 | solution.py:148
  107.2 1.8 fusion.70
  109.0 1.7 fusion.74
  113.2 2.1 convolution_convert_fusion.7
  116.7 3.7 %convolution_convert_fusion.2 = bf16[128,512]{1,0:T(8,128)(2,1)S(1)} fusion(bf16[128,4096]{1,0:T(8,128)(2,1)S(1)} %copy-done.1, bf16[512,4096]{1,0:T(8,128)(2,1)} %param.38), kind=kOutput, calls=%fused_computation.85 | convolution fusion | flops 536936448 | bytes 5373952 | tf_op jit(solution)/shard_map/dot_general | solution.py:60
  122.0 3.1 %convolution_convert_fusion.6 = bf16[128,256]{1,0:T(8,128)(2,1)} fusion(bf16[128,4096]{1,0:T(8,128)(2,1)S(1)} %copy-done.1, bf16[256,4096]{1,0:T(8,128)(2,1)} %param.36), kind=kOutput, calls=%fused_computation.94 | convolution fusion | flops 268468224 | bytes 3211264 | tf_op jit(solution)/shard_map/dot_general | solution.py:60
  128.1 4.4 %convolution_convert_fusion = bf16[128,512]{1,0:T(8,128)(2,1)} fusion(bf16[128,4096]{1,0:T(8,128)(2,1)S(1)} %copy-done.1, bf16[512,4096]{1,0:T(8,128)(2,1)} %param.39), kind=kOutput, calls=%fused_computation.83 | convolution fusion | flops 536936448 | bytes 5373952 | tf_op jit(solution)/shard_map/dot_general | solution.py:60
  138.6 2.3 exponential_multiply_fusion.2
  141.6 5.9 %while.89 = (s32[]{:T(128)}, f32[2,128,256]{2,1,0:T(8,128)S(1)}, f32[2,64,2,256]{3,1,0,2:T(8,128)}, f32[2,64,2,128]{3,2,1,0:T(2,128)S(1)}, f32[2,64,2,128]{3,2,1...) while((s32[]{:T(128)}, f32[2,128,256]{2,1,0:T(8,128)S(1)}, ...), condition=%wide.region_22.23_spmd.clone, body=%wide.region_20.22_spmd.clone.sunk | while | flops 139837440 | bytes 2366588 | solution.py:115
  147.5 1.9 copy.97
  149.4 5.1 %all_gather.44 = bf16[4,2,128]{2,1,0:T(2,128)(2,1)S(1)} all-gather(bf16[1,2,128]{2,1,0:T(2,128)(2,1)} %get-tuple-element.724), channel_id=1, replica_groups=mesh['sp'=4,'tp'=8] {'sp'}, dimensions={0}, use_global_device_ids=true | all-gather | bytes 2560 | tf_op jit(solution)/shard_map/all_gather | solution.py:38
  155.8 7.9 %all-gather.2 = bf16[8,128,256]{2,1,0:T(8,128)(2,1)} all-gather(bf16[2,128,256]{2,1,0:T(8,128)(2,1)S(1)} %convolution_convert_fusion.1), channel_id=4, replica_groups=mesh['sp'=4,'tp'=8] {'sp'}, dimensions={0}, use_global_device_ids=true | all-gather | bytes 655360 | tf_op jit(solution)/shard_map/all_gather | solution.py:38
  163.7 4.4 %while.90 = (s32[]{:T(128)}, f32[2,128]{1,0:T(2,128)S(1)}, f32[2,128,256]{2,1,0:T(8,128)S(1)}, s32[]{:T(128)}, bf16[4,2,128]{2,1,0:T(2,128)(2,1)S(1)}, /*index=5...) while((s32[]{:T(128)}, f32[2,128]{1,0:T(2,128)S(1)}, ...), condition=%wide.region_25.26_spmd.clone, body=%wide.region_24.25_spmd.clone.sunk | while | flops 328968 | bytes 660669 | solution.py:56
  168.1 2.4 fusion.46
  170.5 3.1 %rev.38 = f32[128,2,256]{0,2,1:T(8,128)} reverse(f32[128,2,256]{0,2,1:T(8,128)} %fusion.46), dimensions={0} | reverse | bytes 524288 | tf_op jit(solution)/shard_map/jit(_flip)/rev | solution.py:75
  175.5 4.3 %while.86 = (s32[]{:T(128)}, f32[2,128,256]{2,1,0:T(8,128)S(1)}, f32[2,64,2,256]{3,1,0,2:T(8,128)}, f32[2,64,2,128]{3,2,1,0:T(2,128)S(1)}, f32[2,64,2,128]{3,2,1...) while((s32[]{:T(128)}, f32[2,128,256]{2,1,0:T(8,128)S(1)}, ...), condition=%wide.region_9.10_spmd.clone, body=%wide.region_7.9_spmd.clone.sunk | while | flops 139837440 | bytes 2594944 | solution.py:115
  179.8 1.8 copy.87
  181.6 5.0 %all_gather.39 = bf16[4,2,128]{2,1,0:T(2,128)(2,1)S(1)} all-gather(bf16[1,2,128]{2,1,0:T(2,128)(2,1)S(1)} %get-tuple-element.720), channel_id=1, replica_groups=mesh['sp'=4,'tp'=8] {'sp'}, dimensions={0}, use_global_device_ids=true | all-gather | bytes 2560 | tf_op jit(solution)/shard_map/all_gather | solution.py:38
  187.0 7.6 %all-gather = bf16[8,128,256]{2,1,0:T(8,128)(2,1)S(1)} all-gather(bf16[2,128,256]{2,1,0:T(8,128)(2,1)S(1)} %convolution_convert_fusion.3), channel_id=2, replica_groups=mesh['sp'=4,'tp'=8] {'sp'}, dimensions={0}, use_global_device_ids=true | all-gather | bytes 655360 | tf_op jit(solution)/shard_map/all_gather | solution.py:38
  199.2 36.8 %all-gather.9.cloned.1.call-done = bf16[128,4096]{1,0:T(8,128)(2,1)} async-done(((bf16[128,512]{1,0:T(8,128)(2,1)}), bf16[128,4096]{1,0:T(8,128)(2,1)}) %all-gather.9.cloned.1.call-update) | async-done | bytes 1048592 | tf_op jit(solution)/shard_map/all_gather | solution.py:301
  236.0 4.7 %fusion.50 = bf16[128,512]{1,0:T(8,128)(2,1)} fusion(bf16[128,4096]{1,0:T(8,128)(2,1)} %all-gather.9.cloned.1.call-done, bf16[512,4096]{1,0:T(8,128)(2,1)} %param.45, bf16[128,512]{1,0:T(8,128)(2,1)S(1)} %copy-done.11, f32[512]{0:T(512)S(1)} %bitcast.292), kind=kOutput, calls=%fused_computation.87 | convolution fusion | flops 537133056 | bytes 5507072 | tf_op jit(solution)/shard_map/dot_general | solution.py:60
  (209 shorter events, 66.7 us)
Async XLA Ops:
  6.5 61.6 %copy-start = (bf16[256,4096]{1,0:T(8,128)(2,1)S(1)}, bf16[256,4096]{1,0:T(8,128)(2,1)}, u32[]{:S(2)}) copy-start(bf16[256,4096]{1,0:T(8,128)(2,1)} %param.37) | copy-start | bytes 6291460
  6.5 49.8 %copy-start.16 = (bf16[2,4096,16]{1,2,0:T(8,128)(2,1)S(1)}, bf16[2,4096,16]{1,2,0:T(8,128)(2,1)}, u32[]{:S(2)}) copy-start(bf16[2,4096,16]{1,2,0:T(8,128)(2,1)} %param.40) | copy-start | bytes 786436
  6.5 49.8 %copy-start.17 = (bf16[2,16,2048]{2,1,0:T(8,128)(2,1)S(1)}, bf16[2,16,2048]{2,1,0:T(8,128)(2,1)}, u32[]{:S(2)}) copy-start(bf16[2,16,2048]{2,1,0:T(8,128)(2,1)} %param.41) | copy-start | bytes 393220
  6.5 50.5 %copy-start.18 = (f32[2,2048]{1,0:T(2,128)S(1)}, f32[2,2048]{1,0:T(2,128)}, u32[]{:S(2)}) copy-start(f32[2,2048]{1,0:T(2,128)} %param.42) | copy-start | bytes 49156
  6.5 100.7 %all-gather.7.cloned.1.call-start = ((), (), s32[]{:S(2)}) async-start(), calls=%async_computation.1 | async-start | bytes 1179648 | tf_op jit(solution)/shard_map/all_gather | solution.py:208
  52.9 10.7 %all-to-all-start = ((bf16[8,16,512]{2,1,0:T(8,128)(2,1)}), bf16[8,16,512]{2,1,0:T(8,128)(2,1)S(1)}, u32[]{:S(2)}, u32[]{:S(2)}) async-start(bf16[8,16,512]{2,1,0:T(8,128)(2,1)} %stack.11), calls=%async_computation | async-start | bytes 262144 | tf_op jit(solution)/shard_map/all_to_all | solution.py:19
  56.3 179.7 %all-gather.9.cloned.1.call-start = ((), (), s32[]{:S(2)}) async-start(), calls=%async_computation.2 | async-start | bytes 1179648 | tf_op jit(solution)/shard_map/all_gather | solution.py:301
  56.4 18.8 %copy-start.15 = (bf16[16,4096]{1,0:T(8,128)(2,1)}, bf16[16,4096]{1,0:T(8,128)(2,1)S(1)}, u32[]{:S(2)}) copy-start(bf16[16,4096]{1,0:T(8,128)(2,1)S(1)} %get-tuple-element.713) | copy-start | bytes 393220
  88.0 18.5 %copy-start.5 = (f32[2,128,256]{2,1,0:T(8,128)}, f32[2,128,256]{2,1,0:T(8,128)S(1)}, u32[]{:S(2)}) copy-start(f32[2,128,256]{2,1,0:T(8,128)S(1)} %get-tuple-element.462) | copy-start | bytes 786436
  106.5 0.7 copy-start.3
  107.2 9.4 %copy-start.1 = (bf16[128,4096]{1,0:T(8,128)(2,1)S(1)}, bf16[128,4096]{1,0:T(8,128)(2,1)}, u32[]{:S(2)}) copy-start(bf16[128,4096]{1,0:T(8,128)(2,1)} %all-gather.7.cloned.1.call-done) | copy-start | bytes 3145732
  132.5 9.1 %copy-start.2 = (f32[2,128,256]{2,1,0:T(8,128)S(1)}, f32[2,128,256]{2,1,0:T(8,128)}, u32[]{:S(2)}) copy-start(f32[2,128,256]{2,1,0:T(8,128)} %custom-call.4) | copy-start | bytes 786436
  141.6 22.1 %copy-start.8 = (f32[2,128,256]{2,1,0:T(8,128)S(1)}, f32[2,128,256]{2,1,0:T(8,128)}, u32[]{:S(2)}) copy-start(f32[2,128,256]{2,1,0:T(8,128)} %custom-call.6) | copy-start | bytes 786436
  147.5 20.6 %copy-start.4 = (f32[2,128,256]{2,1,0:T(8,128)S(1)}, f32[2,128,256]{2,1,0:T(8,128)}, u32[]{:S(2)}) copy-start(f32[2,128,256]{2,1,0:T(8,128)} %copy-done.3) | copy-start | bytes 786436
  147.5 28.0 %copy-start.9 = (f32[2,64,2,256]{3,2,1,0:T(2,128)S(1)}, f32[2,64,2,256]{3,2,1,0:T(2,128)}, u32[]{:S(2)}) copy-start(f32[2,64,2,256]{3,2,1,0:T(2,128)} %reshape_reshape.7) | copy-start | bytes 786436
  155.8 17.8 %copy-start.14 = (f32[128,256]{1,0:T(8,128)S(1)}, f32[128,256]{1,0:T(8,128)}, u32[]{:S(2)}) copy-start(f32[128,256]{1,0:T(8,128)} %broadcast_multiply_fusion) | copy-start | bytes 393220
  155.8 19.7 %copy-start.10 = (f32[2,64,2,128]{3,2,1,0:T(2,128)S(1)}, f32[2,64,2,128]{3,2,1,0:T(2,128)}, u32[]{:S(2)}) copy-start(f32[2,64,2,128]{3,2,1,0:T(2,128)} %reshape_reshape.6) | copy-start | bytes 393220
  175.5 11.2 %copy-start.13 = (f32[128,2,128]{2,1,0:T(2,128)S(1)}, f32[128,2,128]{2,1,0:T(2,128)}, u32[]{:S(2)}) copy-start(f32[128,2,128]{2,1,0:T(2,128)} %get-tuple-element.717) | copy-start | bytes 393220
  175.5 19.2 %copy-start.7 = (f32[2,128,256]{2,1,0:T(8,128)S(1)}, f32[2,128,256]{2,1,0:T(8,128)}, u32[]{:S(2)}) copy-start(f32[2,128,256]{2,1,0:T(8,128)} %custom-call.2) | copy-start | bytes 786436
  179.8 15.6 %copy-start.6 = (f32[2,128,256]{2,1,0:T(8,128)S(1)}, f32[2,128,256]{2,1,0:T(8,128)}, u32[]{:S(2)}) copy-start(f32[2,128,256]{2,1,0:T(8,128)} %copy-done.5) | copy-start | bytes 786436
  179.8 17.7 %copy-start.19 = (f32[512]{0:T(512)S(1)}, f32[512]{0:T(512)}, u32[]{:S(2)}) copy-start(f32[512]{0:T(512)} %param.44) | copy-start | bytes 6148
  187.0 8.4 %copy-start.12 = (f32[128,2,256]{0,2,1:T(8,128)S(1)}, f32[128,2,256]{0,2,1:T(8,128)}, u32[]{:S(2)}) copy-start(f32[128,2,256]{0,2,1:T(8,128)} %rev.38) | copy-start | bytes 786436
  187.0 12.2 %copy-start.20 = (f32[2,512]{1,0:T(2,128)S(1)}, f32[2,512]{1,0:T(2,128)}, u32[]{:S(2)}) copy-start(f32[2,512]{1,0:T(2,128)} %get-tuple-element.705) | copy-start | bytes 12292
  187.0 49.0 %copy-start.11 = (bf16[128,512]{1,0:T(8,128)(2,1)S(1)}, bf16[128,512]{1,0:T(8,128)(2,1)}, u32[]{:S(2)}) copy-start(bf16[128,512]{1,0:T(8,128)(2,1)} %param.29) | copy-start | bytes 393220
Sparse Core Ops, SparseCore 0:
  51.5 36.7 all-gather.6
  199.3 36.6 all-gather.8
